TPU v7x, 32 devices: a whole 2x2x4 slice. The times are simulated.
32 devices in a mesh: sp: 8 (over z, y), tp: 4 (over x, core).
Axes of the slice: x: 2, y: 2, z: 4, core: 2. Of those that a mesh axis runs over, the one named last changes fastest.
Arguments:
- out_grad: bfloat16 [1024, 2048], P('sp', 'tp'), may hold values from -6 to 6
- route_ids: int32 [1024, 2], P('sp'), may hold values from 0 to 7, as said below
- route_weight: float32 [1024, 2], P('sp'), may hold values from 0.1 to 0.9
- expert_inputs: bfloat16 [8, 512, 2048], P('sp'), may hold values from -6 to 6
- gate_weight: bfloat16 [8, 2048, 3072], P('sp', None, 'tp'), may hold values from -0.125 to 0.125
- up_weight: bfloat16 [8, 2048, 3072], P('sp', None, 'tp'), may hold values from -0.125 to 0.125
- down_weight: bfloat16 [8, 3072, 2048], P('sp', 'tp'), may hold values from -0.109375 to 0.109375
- out_gate: bfloat16 [1024, 2048], P('sp', 'tp'), may hold values from -6 to 6
- in_gate: bfloat16 [1024, 2048], P('sp', 'tp'), may hold values from -6 to 6
- values: bfloat16 [1024, 2048], P('sp', 'tp'), may hold values from -6 to 6
- conv_out: bfloat16 [1024, 2048], P('sp', 'tp'), may hold values from -6 to 6
- conv_taps: bfloat16 [3, 2048], P(None, 'tp'), may hold values from -3.5 to 3.5
- proj_weight: bfloat16 [2048, 2048], P(None, 'tp'), may hold values from -0.125 to 0.125
Outputs:
- resid_grad: bfloat16 [1024, 2048], P('sp', 'tp')
- out_gate_grad: bfloat16 [1024, 2048], P('sp', 'tp')
- in_gate_grad: bfloat16 [1024, 2048], P('sp', 'tp')
- values_grad: bfloat16 [1024, 2048], P('sp', 'tp')
- proj_grad: float32 [2048, 2048], P('sp', 'tp')
- gate_grad: bfloat16 [8, 2048, 3072], P('sp', None, 'tp')
- up_grad: bfloat16 [8, 2048, 3072], P('sp', None, 'tp')
- down_grad: bfloat16 [8, 3072, 2048], P('sp', 'tp')
Inputs may be any that keep to these rules, and one draw needn't show every extreme that they name: `route_ids`: each row names two different experts. Among the rows of one device (aligned blocks of 128 rows) no expert is named more than 64 times, and in every draw one expert is named exactly 64 times in every block.
All inputs are finite; a program needn't handle non-finite values.
Results may differ from a plain program's by a relative error of at most 0.017.
Values may be sent and summed in bfloat16 or wider, within the bound.
A program may use at most 128 MiB of HBM per device.

v0:
```python
import math
import jax
import jax.numpy as jnp
from jax import lax
from jax.sharding import PartitionSpec as P


def extended(x, sides, width):
    for axis, dim in sides:
        devices, length = (lax.axis_size(axis), x.shape[dim])
        up = [(i, (i + 1) % devices) for i in range(devices - 1)]
        down = [(j, i) for i, j in up]
        last = lax.slice_in_dim(x, length - width, length, axis=dim)
        first = lax.slice_in_dim(x, 0, width, axis=dim)
        before = lax.ppermute(last, axis, up)
        after = lax.ppermute(first, axis, down)
        x = jnp.concatenate([before, x, after], axis=dim)
    return x


def contract_first(left, right):
    return lax.dot_general(
        left, right, (((0,), (0,)), ((), ())), preferred_element_type=jnp.float32
    )


def contract_last(left, right):
    return lax.dot_general(
        left, right, (((1,), (1,)), ((), ())), preferred_element_type=jnp.float32
    )


def expert_backward(inputs, routed, gate_w, up_w, down_w):
    pre_gate = jnp.dot(inputs, gate_w, preferred_element_type=jnp.float32)
    pre_up = jnp.dot(inputs, up_w, preferred_element_type=jnp.float32)
    sigmoid_g = jax.nn.sigmoid(pre_gate)
    activated = pre_gate * sigmoid_g
    hidden = (activated * pre_up).astype(jnp.bfloat16)
    d_hidden = contract_last(routed, down_w)
    d_gate = (d_hidden * pre_up * sigmoid_g * (1.0 + pre_gate * (1.0 - sigmoid_g))).astype(
        jnp.bfloat16
    )
    d_up = (d_hidden * activated).astype(jnp.bfloat16)
    partial_value = contract_last(d_gate, gate_w) + contract_last(d_up, up_w)
    grad_set = (
        contract_first(inputs, d_gate),
        contract_first(inputs, d_up),
        contract_first(hidden, routed),
    )
    return (partial_value, grad_set)


def expert_pass(outgoing, input_rows, gate_weight, up_weight, down_weight):
    arrived = lax.all_to_all(outgoing, "sp", split_axis=0, concat_axis=1, tiled=True)
    routed = lax.all_gather(arrived, "tp", axis=2, tiled=True)
    partial_value, grad_set = expert_backward(
        input_rows[0], routed[0], gate_weight[0], up_weight[0], down_weight[0]
    )
    partials = [partial_value]
    gate_list = [grad_set[0]]
    up_list = [grad_set[1]]
    down_list = [grad_set[2]]
    summed = lax.psum_scatter(
        jnp.stack(partials).astype(jnp.bfloat16), "tp", scatter_dimension=2, tiled=True
    )
    returned = lax.all_to_all(summed, "sp", split_axis=1, concat_axis=0, tiled=True)
    return (returned, (jnp.stack(gate_list), jnp.stack(up_list), jnp.stack(down_list)))


def per_device(
    out_grad,
    route_ids,
    route_weight,
    expert_inputs,
    gate_weight,
    up_weight,
    down_weight,
    out_gate,
    in_gate,
    values,
    conv_out,
    conv_taps,
    proj_weight,
):
    sp_devices = lax.axis_size("sp")
    tok_rows = out_grad.shape[0]
    local_experts = gate_weight.shape[0]
    all_experts = sp_devices * local_experts
    capacity = 4 * tok_rows // all_experts
    flat_ids = route_ids.reshape(-1)
    onehot = (flat_ids[:, None] == jnp.arange(all_experts, dtype=jnp.int32)[None, :]).astype(
        jnp.int32
    )
    ranked = jnp.sum((jnp.cumsum(onehot, axis=0) - onehot) * onehot, axis=1)
    slot_ids = flat_ids * capacity + ranked
    dispatch = (
        jnp.arange(all_experts * capacity, dtype=jnp.int32)[:, None] == slot_ids[None, :]
    ).astype(jnp.bfloat16)
    weighted = (
        (route_weight[:, :, None] * out_grad.astype(jnp.float32)[:, None, :])
        .astype(jnp.bfloat16)
        .reshape(2 * tok_rows, -1)
    )
    outgoing = jnp.dot(dispatch, weighted, preferred_element_type=jnp.float32).astype(jnp.bfloat16)
    outgoing = outgoing.reshape(all_experts, capacity, -1)
    returned, totals = expert_pass(outgoing, expert_inputs, gate_weight, up_weight, down_weight)
    slot_scale = 1.0 / math.sqrt(expert_inputs.shape[1])
    gate_grad = (totals[0] * slot_scale).astype(jnp.bfloat16)
    up_grad = (totals[1] * slot_scale).astype(jnp.bfloat16)
    down_grad = (totals[2] * slot_scale).astype(jnp.bfloat16)
    combiner = jnp.sum(dispatch.reshape(all_experts * capacity, tok_rows, 2), axis=2)
    moe_part = contract_first(combiner, returned.reshape(all_experts * capacity, -1))
    resid_grad = (out_grad.astype(jnp.float32) + moe_part).astype(jnp.bfloat16)
    resid_full = lax.all_gather(resid_grad, "tp", axis=1, tiled=True)
    mix_grad = jnp.dot(resid_full, proj_weight, preferred_element_type=jnp.float32)
    gate_vals = out_gate.astype(jnp.float32)
    conv_vals = conv_out.astype(jnp.float32)
    mixed_in = (gate_vals * conv_vals).astype(jnp.bfloat16)
    out_gate_grad = (mix_grad * conv_vals).astype(jnp.bfloat16)
    conv_grad = (mix_grad * gate_vals).astype(jnp.bfloat16)
    padded = extended(conv_grad, (("sp", 0),), 1).astype(jnp.float32)
    tap_vals = conv_taps.astype(jnp.float32)
    value_grad = padded[2:] * tap_vals[0] + padded[1:-1] * tap_vals[1] + padded[:-2] * tap_vals[2]
    in_gate_grad = (value_grad * values.astype(jnp.float32)).astype(jnp.bfloat16)
    values_grad = (value_grad * in_gate.astype(jnp.float32)).astype(jnp.bfloat16)
    token_scale = 1.0 / math.sqrt(tok_rows * sp_devices)
    columns = lax.all_to_all(resid_full, "sp", split_axis=1, concat_axis=0, tiled=True)
    proj_sum = contract_first(columns, lax.all_gather(mixed_in, "sp", axis=0, tiled=True))
    proj_grad = proj_sum * token_scale
    return (
        resid_grad,
        out_gate_grad,
        in_gate_grad,
        values_grad,
        proj_grad,
        gate_grad,
        up_grad,
        down_grad,
    )


def solution(mesh):
    in_specs = (
        P("sp", "tp"),
        P("sp", None),
        P("sp", None),
        P("sp", None, None),
        P("sp", None, "tp"),
        P("sp", None, "tp"),
        P("sp", "tp", None),
        P("sp", "tp"),
        P("sp", "tp"),
        P("sp", "tp"),
        P("sp", "tp"),
        P(None, "tp"),
        P(None, "tp"),
    )
    out_specs = (
        P("sp", "tp"),
        P("sp", "tp"),
        P("sp", "tp"),
        P("sp", "tp"),
        P("sp", "tp"),
        P("sp", None, "tp"),
        P("sp", None, "tp"),
        P("sp", "tp", None),
    )
    return jax.shard_map(
        per_device, mesh=mesh, in_specs=in_specs, out_specs=out_specs, check_vma=False
    )
```

profile of v0, /device:TPU:0, one launch (start us, length us, event | category | flops | bytes accessed | tf_op | source)
XLA Modules:
  0.0 198.5 jit_solution(15342331069827276)
XLA Ops:
  15.8 21.7 %all_to_all.40 = bf16[8,64,512]{2,1,0:T(8,128)(2,1)} all-to-all(bf16[8,64,512]{2,1,0:T(8,128)(2,1)S(1)} %bitcast.88), channel_id=1, replica_groups=mesh['sp'=8,'tp'=4] {'sp'}, dimensions={0} | all-to-all | bytes 1048576 | tf_op jit(solution)/shard_map/all_to_all | solution.py:54
  37.6 4.7 %fusion.2 = f32[512,768]{1,0:T(8,128)} fusion(bf16[1,2048,768]{2,1,0:T(8,128)(2,1)S(1)} %copy-done, bf16[1,512,2048]{2,1,0:T(8,128)(2,1)} %param.16), kind=kOutput, calls=%fused_computation.6 | convolution fusion | flops 1610612736 | bytes 6815744 | tf_op jit(solution)/shard_map/dot_general | solution.py:34
  42.3 3.0 %fusion.6 = f32[512,768]{1,0:T(8,128)} fusion(bf16[1,2048,768]{2,1,0:T(8,128)(2,1)S(1)} %copy-done.9, bf16[1,512,2048]{2,1,0:T(8,128)(2,1)S(1)} %copy-done.11), kind=kOutput, calls=%fused_computation.10 | convolution fusion | flops 1610612736 | bytes 6815744 | tf_op jit(solution)/shard_map/dot_general | solution.py:35
  45.3 14.0 %all-gather.3.cloned.1.call-done = bf16[1,512,2048]{2,1,0:T(8,128)(2,1)} async-done(((bf16[1,512,512]{2,1,0:T(8,128)(2,1)}), bf16[1,512,2048]{2,1,0:T(8,128)(2,1)}) %all-gather.3.cloned.1.call-update) | async-done | bytes 2097168 | tf_op jit(solution)/shard_map/all_gather | solution.py:55
  59.3 5.6 %multiply_convert_fusion.4 = (bf16[512,768]{1,0:T(8,128)(2,1)S(1)}, bf16[512,768]{1,0:T(8,128)(2,1)S(1)}) fusion(f32[512,768]{1,0:T(8,128)} %fusion.2, f32[512,768]{1,0:T(8,128)} %fusion.6, bf16[1,768,2048]{2,1,0:T(8,128)(2,1)} %param.19, bf16[1,512,2048]{2,1,0:T(8,128)(2,1)} %all-gather.3.cloned.1.call-done), kind=kOutput, calls=%fused_computation.25 | convolution fusion | flops 1615724544 | bytes 9961472 | tf_op jit(solution)/shard_map/dot_general | solution.py:28
  67.4 3.1 %fusion.15 = bf16[1,512,2048]{2,1,0:T(8,128)(2,1)} fusion(f32[512,2048]{1,0:T(8,128)S(1)} %fusion, bf16[512,768]{1,0:T(8,128)(2,1)S(1)} %get-tuple-element.58, bf16[1,2048,768]{2,1,0:T(8,128)(2,1)S(1)} %copy-done.10), kind=kOutput, calls=%fused_computation.17 | convolution fusion | flops 1612709888 | bytes 10223616 | tf_op jit(solution)/shard_map/dot_general | solution.py:28
  70.8 31.1 %reduce-scatter.2.cloned.1.call-done = bf16[1,512,512]{2,1,0:T(8,128)(2,1)} async-done(((bf16[1,512,2048]{2,1,0:T(8,128)(2,1)}), bf16[1,512,512]{2,1,0:T(8,128)(2,1)}) %reduce-scatter.2.cloned.1.call-update) | async-done | bytes 524304 | tf_op jit(solution)/shard_map/reduce_scatter | solution.py:63
  101.9 2.8 %copy.77 = bf16[1,512,512]{2,0,1:T(2,128)(2,1)} copy(bf16[1,512,512]{2,1,0:T(8,128)(2,1)} %reduce-scatter.2.cloned.1.call-done) | data formatting | bytes 1048576 | tf_op jit(solution)/shard_map/reduce_scatter | solution.py:63
  105.2 5.6 %reduce.3 = bf16[512,512]{1,0:T(8,128)(2,1)} reduce(bf16[512,1,512]{2,1,0:T(2,128)(2,1)} %bitcast.84, bf16[]{:T(256)} %broadcast.62), dimensions={1}, to_apply=%bitcast.82.reduce_sub_computation | reduce | bytes 1048578
  110.8 2.2 %reshape.85 = bf16[8,2,16384]{2,1,0:T(2,128)(2,1)} reshape(bf16[512,512]{1,0:T(8,128)(2,1)} %reduce.3) | data formatting | bytes 1048576
  113.0 5.5 %all-to-all-start.1 = ((bf16[8,2,16384]{2,1,0:T(2,128)(2,1)}), bf16[8,2,16384]{2,1,0:T(2,128)(2,1)}, u32[]{:S(2)}, u32[]{:S(2)}) async-start(bf16[8,2,16384]{2,1,0:T(2,128)(2,1)} %reshape.85), calls=%async_computation.2 | async-start | bytes 1048576 | tf_op jit(solution)/shard_map/all_to_all | solution.py:66
  118.9 5.4 %fusion.10 = bf16[1,2048,768]{1,2,0:T(8,128)(2,1)} fusion(bf16[512,768]{1,0:T(8,128)(2,1)} %copy-done.13, bf16[1,512,2048]{2,1,0:T(8,128)(2,1)} %param.16), kind=kOutput, calls=%fused_computation.14 | convolution fusion | flops 1613758464 | bytes 6029312 | tf_op jit(solution)/shard_map/dot_general | solution.py:22
  124.2 8.7 %all-to-all-done.1 = bf16[8,2,16384]{2,1,0:T(2,128)(2,1)} async-done(((bf16[8,2,16384]{2,1,0:T(2,128)(2,1)}), bf16[8,2,16384]{2,1,0:T(2,128)(2,1)}, u32[]{:S(2)}, u32[]{:S(2)}) %all-to-all-start.1) | async-done | bytes 524320 | tf_op jit(solution)/shard_map/all_to_all | solution.py:66
  132.9 3.5 %reshape.86 = bf16[512,1,512]{2,1,0:T(2,128)(2,1)} reshape(bf16[8,2,16384]{2,1,0:T(2,128)(2,1)} %all-to-all-done.1) | data formatting | bytes 1048576
  137.9 6.5 %all_gather.10 = bf16[128,2048]{1,0:T(8,128)(2,1)S(1)} all-gather(bf16[128,512]{1,0:T(8,128)(2,1)S(1)} %fusion.25), channel_id=1, replica_groups=mesh['sp'=8,'tp'=4] {'tp'}, dimensions={1}, use_global_device_ids=true | all-gather | bytes 655360 | tf_op jit(solution)/shard_map/all_gather | solution.py:114
  145.2 2.8 %fusion.31 = (bf16[128,512]{1,0:T(8,128)(2,1)S(1)}, bf16[128,512]{1,0:T(8,128)(2,1)}, bf16[128,512]{1,0:T(8,128)(2,1)}) fusion(bf16[128,512]{1,0:T(8,128)(2,1)} %param.20, bf16[128,512]{1,0:T(8,128)(2,1)} %param.23, bf16[128,2048]{1,0:T(8,128)(2,1)S(1)} %all_gather.10, bf16[2048,512]{1,0:T(8,128)(2,1)} %param.25), kind=kOutput, calls=%fused_computation.44 | convolution fusion | flops 268959744 | bytes 3276800 | tf_op jit(solution)/shard_map/dot_general | solution.py:115
  148.0 6.1 %fusion.12 = bf16[1,768,2048]{2,1,0:T(8,128)(2,1)} fusion(bf16[1,512,2048]{2,1,0:T(8,128)(2,1)} %all-gather.3.cloned.1.call-done, f32[512,768]{1,0:T(8,128)} %fusion.6, f32[512,768]{1,0:T(8,128)} %fusion.2), kind=kOutput, calls=%fused_computation.16 | convolution fusion | flops 1616117760 | bytes 8388608 | tf_op jit(solution)/shard_map/dot_general | solution.py:22
  154.8 3.4 %collective-permute-start = (bf16[1,512]{1,0:T(2,128)(2,1)}, bf16[1,512]{1,0:T(2,128)(2,1)S(1)}, u32[]{:S(2)}, u32[]{:S(2)}) collective-permute-start(bf16[1,512]{1,0:T(2,128)(2,1)} %get-tuple-element.63), channel_id=1, source_target_pairs={{0,4},{4,8},{8,12},{12,16},{16,20},{20,24},{24,28},{1,5},{5,9},{9,... | collective-permute-start | bytes 3080 | tf_op jit(solution)/shard_map/ppermute | solution.py:15
  160.3 5.8 %all-to-all-start.2 = ((bf16[128,8,256]{2,0,1:T(8,128)(2,1)}), bf16[128,8,256]{2,0,1:T(8,128)(2,1)}, u32[]{:S(2)}, u32[]{:S(2)}) async-start(bf16[128,8,256]{2,0,1:T(8,128)(2,1)} %bitcast.86), calls=%async_computation.3 | async-start | bytes 1048576 | tf_op jit(solution)/shard_map/all_to_all | solution.py:127
  166.0 5.3 %fusion.11 = bf16[1,2048,768]{1,2,0:T(8,128)(2,1)} fusion(bf16[512,768]{1,0:T(8,128)(2,1)} %copy-done.12, bf16[1,512,2048]{2,1,0:T(8,128)(2,1)} %param.16), kind=kOutput, calls=%fused_computation.15 | convolution fusion | flops 1613758464 | bytes 6029312 | tf_op jit(solution)/shard_map/dot_general | solution.py:22
  171.3 4.6 %copy.66 = bf16[1,2048,768]{2,1,0:T(8,128)(2,1)} copy(bf16[1,2048,768]{1,2,0:T(8,128)(2,1)} %fusion.10) | data formatting | bytes 6291456
  176.0 4.7 %copy.67 = bf16[1,2048,768]{2,1,0:T(8,128)(2,1)} copy(bf16[1,2048,768]{1,2,0:T(8,128)(2,1)} %fusion.11) | data formatting | bytes 6291456
  182.8 5.7 %all-to-all-done.2 = bf16[128,8,256]{2,0,1:T(8,128)(2,1)} async-done(((bf16[128,8,256]{2,0,1:T(8,128)(2,1)}), bf16[128,8,256]{2,0,1:T(8,128)(2,1)}, u32[]{:S(2)}, u32[]{:S(2)}) %all-to-all-start.2) | async-done | bytes 524320 | tf_op jit(solution)/shard_map/all_to_all | solution.py:127
  189.3 2.6 %convolution_multiply_fusion = f32[256,512]{1,0:T(8,128)} fusion(bf16[1024,256]{1,0:T(8,128)(2,1)} %bitcast.14, bf16[1024,512]{1,0:T(8,128)(2,1)} %all-gather.5.cloned.1.call-done), kind=kOutput, calls=%fused_computation.30 | convolution fusion | flops 268566528 | bytes 2097152 | tf_op jit(solution)/shard_map/dot_general | solution.py:22
  (66 shorter events, 20.1 us)
Async XLA Ops:
  7.2 30.4 %copy-start = (bf16[1,2048,768]{2,1,0:T(8,128)(2,1)S(1)}, bf16[1,2048,768]{2,1,0:T(8,128)(2,1)}, u32[]{:S(2)}) copy-start(bf16[1,2048,768]{2,1,0:T(8,128)(2,1)} %param.17) | copy-start | bytes 9437188
  7.2 52.1 %all-gather.3.cloned.1.call-start = ((), (), s32[]{:S(2)}) async-start(), calls=%async_computation.4 | async-start | bytes 2621440 | tf_op jit(solution)/shard_map/all_gather | solution.py:55
  37.6 64.3 %reduce-scatter.2.cloned.1.call-start = ((), (), s32[]{:S(2)}) async-start(), calls=%async_computation.5 | async-start | bytes 2621440 | tf_op jit(solution)/shard_map/reduce_scatter | solution.py:63
  37.6 4.7 %copy-start.9 = (bf16[1,2048,768]{2,1,0:T(8,128)(2,1)S(1)}, bf16[1,2048,768]{2,1,0:T(8,128)(2,1)}, u32[]{:S(2)}) copy-start(bf16[1,2048,768]{2,1,0:T(8,128)(2,1)} %param.18) | copy-start | bytes 9437188
  37.6 4.7 %copy-start.11 = (bf16[1,512,2048]{2,1,0:T(8,128)(2,1)S(1)}, bf16[1,512,2048]{2,1,0:T(8,128)(2,1)}, u32[]{:S(2)}) copy-start(bf16[1,512,2048]{2,1,0:T(8,128)(2,1)} %param.16) | copy-start | bytes 6291460
  64.9 1.9 copy-start.13
  64.9 1.9 copy-start.12
  64.9 2.5 %copy-start.10 = (bf16[1,2048,768]{2,1,0:T(8,128)(2,1)S(1)}, bf16[1,2048,768]{2,1,0:T(8,128)(2,1)}, u32[]{:S(2)}) copy-start(bf16[1,2048,768]{2,1,0:T(8,128)(2,1)} %param.18) | copy-start | bytes 9437188
  104.7 14.0 %copy-start.8 = (s32[128,2]{0,1:T(2,128)S(1)}, s32[128,2]{0,1:T(2,128)}, u32[]{:S(2)}) copy-start(s32[128,2]{0,1:T(2,128)} %param.14) | copy-start | bytes 3076
  104.7 14.1 %copy-start.7 = (bf16[3,512]{1,0:T(4,128)(2,1)S(1)}, bf16[3,512]{1,0:T(4,128)(2,1)}, u32[]{:S(2)}) copy-start(bf16[3,512]{1,0:T(4,128)(2,1)} %param.24) | copy-start | bytes 9220
  113.0 19.9 %all-to-all-start.1 = ((bf16[8,2,16384]{2,1,0:T(2,128)(2,1)}), bf16[8,2,16384]{2,1,0:T(2,128)(2,1)}, u32[]{:S(2)}, u32[]{:S(2)}) async-start(bf16[8,2,16384]{2,1,0:T(2,128)(2,1)} %reshape.85), calls=%async_computation.2 | async-start | bytes 1048576 | tf_op jit(solution)/shard_map/all_to_all | solution.py:66
  118.5 70.8 %all-gather.5.cloned.1.call-start = ((), (), s32[]{:S(2)}) async-start(), calls=%async_computation.6 | async-start | bytes 1179648 | tf_op jit(solution)/shard_map/all_gather | solution.py:128
  118.8 17.6 %copy-start.3 = (bf16[128,512]{1,0:T(8,128)(2,1)S(1)}, bf16[128,512]{1,0:T(8,128)(2,1)}, u32[]{:S(2)}) copy-start(bf16[128,512]{1,0:T(8,128)(2,1)} %param.13) | copy-start | bytes 393220
  137.9 16.3 %copy-start.4 = (bf16[128,512]{1,0:T(8,128)(2,1)}, bf16[128,512]{1,0:T(8,128)(2,1)S(1)}, u32[]{:S(2)}) copy-start(bf16[128,512]{1,0:T(8,128)(2,1)S(1)} %fusion.25) | copy-start | bytes 393220
  144.4 0.8 copy-start.1
  148.0 11.4 %copy-start.2 = (bf16[128,2048]{1,0:T(8,128)(2,1)S(1)}, bf16[128,2048]{1,0:T(8,128)(2,1)}, u32[]{:S(2)}) copy-start(bf16[128,2048]{1,0:T(8,128)(2,1)} %copy-done.1) | copy-start | bytes 1572868
  154.8 25.9 %collective-permute-start = (bf16[1,512]{1,0:T(2,128)(2,1)}, bf16[1,512]{1,0:T(2,128)(2,1)S(1)}, u32[]{:S(2)}, u32[]{:S(2)}) collective-permute-start(bf16[1,512]{1,0:T(2,128)(2,1)} %get-tuple-element.63), channel_id=1, source_target_pairs={{0,4},{4,8},{8,12},{12,16},{16,20},{20,24},{24,28},{1,5},{5,9},{9,... | collective-permute-start | bytes 3080 | tf_op jit(solution)/shard_map/ppermute | solution.py:15
  158.1 22.5 %collective-permute-start.1 = (bf16[1,512]{1,0:T(2,128)(2,1)}, bf16[1,512]{1,0:T(2,128)(2,1)}, u32[]{:S(2)}, u32[]{:S(2)}) collective-permute-start(bf16[1,512]{1,0:T(2,128)(2,1)} %get-tuple-element.64), channel_id=1, source_target_pairs={{4,0},{8,4},{12,8},{16,12},{20,16},{24,20},{28,24},{5,1},{9,5},{13... | collective-permute-start | bytes 3080 | tf_op jit(solution)/shard_map/ppermute | solution.py:16
  160.3 28.2 %all-to-all-start.2 = ((bf16[128,8,256]{2,0,1:T(8,128)(2,1)}), bf16[128,8,256]{2,0,1:T(8,128)(2,1)}, u32[]{:S(2)}, u32[]{:S(2)}) async-start(bf16[128,8,256]{2,0,1:T(8,128)(2,1)} %bitcast.86), calls=%async_computation.3 | async-start | bytes 1048576 | tf_op jit(solution)/shard_map/all_to_all | solution.py:127
  176.0 5.4 %copy-start.5 = (bf16[128,512]{1,0:T(8,128)(2,1)S(1)}, bf16[128,512]{1,0:T(8,128)(2,1)}, u32[]{:S(2)}) copy-start(bf16[128,512]{1,0:T(8,128)(2,1)} %param.21) | copy-start | bytes 393220
  176.0 6.2 %copy-start.6 = (bf16[128,512]{1,0:T(8,128)(2,1)S(1)}, bf16[128,512]{1,0:T(8,128)(2,1)}, u32[]{:S(2)}) copy-start(bf16[128,512]{1,0:T(8,128)(2,1)} %param.22) | copy-start | bytes 393220
Sparse Core Ops, SparseCore 0:
  37.7 21.5 all-gather.2
  70.7 31.1 reduce-scatter.1
  148.1 41.1 all-gather.4
where the time goes:
time: 200 us; the launch traced here: 198 us
  waiting for transfers between devices  60.4 us (30%)
  matrix products  43.4 us (22%)
  blocking collectives  28.2 us (14%)
  local copies, waits for them, and re-layouts  27.8 us (14%)
  starting transfers between devices  16.2 us (8%)
  between operations  14 us (7%)
  other arithmetic  8.51 us (4%)
    reduce_scatter x1, waiting for transfers between devices, expert_pass(): lax.psum_scatter(jnp.stack(partials).astype(jnp.bfloat16), 'tp', scatter_...  31.1 us
    all_to_all x1, blocking collectives, expert_pass(): lax.all_to_all(outgoing, 'sp', split_axis=0, concat_axis=1, tiled=True)  21.7 us
    dot_general x5, matrix products, contract_first(): lax.dot_general(left, right, (((0,), (0,)), ((), ())), preferred_element_...  20.9 us
    unnamed x35, local copies, waits for them, and re-layouts  18.7 us
    all_gather x1, waiting for transfers between devices, expert_pass(): routed = lax.all_gather(arrived, 'tp', axis=2, tiled=True)  14 us
    dot_general x3, matrix products, contract_last(): lax.dot_general(left, right, (((1,), (1,)), ((), ())), preferred_element_...  10.6 us
    all_to_all x1, waiting for transfers between devices, expert_pass(): lax.all_to_all(summed, 'sp', split_axis=1, concat_axis=0, tiled=True)  8.71 us
    all_gather x1, blocking collectives, per_device(): resid_full = lax.all_gather(resid_grad, 'tp', axis=1, tiled=True)  6.5 us
  transfers between devices with their start and end apart: 7, of which 5 were waited for; matrix products, arithmetic and copies ran while one was open for 19% of the time, Pallas kernels for 0%

commit v1 on v0

--- a/solution.py
+++ b/solution.py
@@ -63,7 +63,15 @@
     summed = lax.psum_scatter(
         jnp.stack(partials).astype(jnp.bfloat16), "tp", scatter_dimension=2, tiled=True
     )
-    returned = lax.all_to_all(summed, "sp", split_axis=1, concat_axis=0, tiled=True)
+    returned = jnp.concatenate(
+        lax.all_to_all(
+            jnp.stack(jnp.split(summed, lax.axis_size("sp"), 1), 0),
+            "sp",
+            split_axis=0,
+            concat_axis=0,
+        ),
+        0,
+    )
     return (returned, (jnp.stack(gate_list), jnp.stack(up_list), jnp.stack(down_list)))
 
 

time: 200 us -> 199 us (level)
  other arithmetic: 8.51 us -> 2.95 us
  local copies, waits for them, and re-layouts: 27.8 us -> 30.7 us
  waiting for transfers between devices: 60.4 us -> 63.3 us
    all_gather x1, waiting for transfers between devices: 0.82 us -> 9.29 us  [per_device(): lax.all_gather(mixed_in, 'sp', axis=0, tiled=True)]
    all_to_all x1, waiting for transfers between devices: 5.67 us -> 0.01 us  [per_device(): lax.all_to_all(resid_full, 'sp', split_axis=1, concat_axis=0, tiled=True)]
    unnamed x1 -> x0, other arithmetic: 5.56 us -> none
    unnamed x35 -> x39, local copies, waits for them, and re-layouts: 18.7 us -> 22.9 us
    reduce_scatter x1 -> x0, local copies, waits for them, and re-layouts: 2.82 us -> none  [expert_pass(): lax.psum_scatter(jnp.stack(partials).astype(jnp.bfloat16), 'tp', scatter_...]
  transfers between devices with their start and end apart: 7 -> 7, of which waited for: 5 -> 4; matrix products, arithmetic and copies ran while one was open for 19% -> 19% of each run, Pallas kernels for 0% -> 0%
where the time goes in v1:
time: 199 us; the launch traced here: 197 us
  waiting for transfers between devices  63.3 us (32%)
  matrix products  43.2 us (22%)
  local copies, waits for them, and re-layouts  30.7 us (15%)
  blocking collectives  28.4 us (14%)
  starting transfers between devices  14.9 us (7%)
  between operations  14 us (7%)
  other arithmetic  2.95 us (1%)
    reduce_scatter x1, waiting for transfers between devices, expert_pass(): lax.psum_scatter(jnp.stack(partials).astype(jnp.bfloat16), 'tp', scatter_...  31.1 us
    unnamed x39, local copies, waits for them, and re-layouts  22.9 us
    all_to_all x1, blocking collectives, expert_pass(): lax.all_to_all(outgoing, 'sp', split_axis=0, concat_axis=1, tiled=True)  21.7 us
    dot_general x5, matrix products, contract_first(): lax.dot_general(left, right, (((0,), (0,)), ((), ())), preferred_element_...  20.8 us
    all_gather x1, waiting for transfers between devices, expert_pass(): routed = lax.all_gather(arrived, 'tp', axis=2, tiled=True)  14 us
    dot_general x3, matrix products, contract_last(): lax.dot_general(left, right, (((1,), (1,)), ((), ())), preferred_element_...  10.6 us
    all_gather x1, waiting for transfers between devices, per_device(): lax.all_gather(mixed_in, 'sp', axis=0, tiled=True)  9.29 us
    all_to_all x1, waiting for transfers between devices, expert_pass(): lax.all_to_all(jnp.stack(jnp.split(summed, lax.axis_size('sp'), 1), 0), '...  8.89 us
  transfers between devices with their start and end apart: 7, of which 4 were waited for; matrix products, arithmetic and copies ran while one was open for 19% of the time, Pallas kernels for 0%

profile of v1, /device:TPU:0, one launch (start us, length us, event | category | flops | bytes accessed | tf_op | source)
XLA Modules:
  0.0 197.4 jit_solution(2162120262785751519)
XLA Ops:
  9.4 1.8 mul.130
  11.2 2.2 %mul.131 = f32[256,512]{1,0:T(8,128)} reshape(f32[128,2,512]{2,1,0:T(2,128)} %mul.130) | data formatting | bytes 1048576 | tf_op jit(solution)/shard_map/mul | solution.py:108
  15.8 21.7 %all_to_all.36 = bf16[8,64,512]{2,1,0:T(8,128)(2,1)} all-to-all(bf16[8,64,512]{2,1,0:T(8,128)(2,1)S(1)} %bitcast.113), channel_id=1, replica_groups=mesh['sp'=8,'tp'=4] {'sp'}, dimensions={0} | all-to-all | bytes 1048576 | tf_op jit(solution)/shard_map/all_to_all | solution.py:54
  37.6 4.7 %fusion.2 = f32[512,768]{1,0:T(8,128)} fusion(bf16[1,2048,768]{2,1,0:T(8,128)(2,1)S(1)} %copy-done, bf16[1,512,2048]{2,1,0:T(8,128)(2,1)} %param.16), kind=kOutput, calls=%fused_computation.6 | convolution fusion | flops 1610612736 | bytes 6815744 | tf_op jit(solution)/shard_map/dot_general | solution.py:34
  42.3 3.0 %fusion.6 = f32[512,768]{1,0:T(8,128)} fusion(bf16[1,2048,768]{2,1,0:T(8,128)(2,1)S(1)} %copy-done.9, bf16[1,512,2048]{2,1,0:T(8,128)(2,1)S(1)} %copy-done.11), kind=kOutput, calls=%fused_computation.10 | convolution fusion | flops 1610612736 | bytes 6815744 | tf_op jit(solution)/shard_map/dot_general | solution.py:35
  45.3 14.0 %all-gather.3.cloned.1.call-done = bf16[1,512,2048]{2,1,0:T(8,128)(2,1)} async-done(((bf16[1,512,512]{2,1,0:T(8,128)(2,1)}), bf16[1,512,2048]{2,1,0:T(8,128)(2,1)}) %all-gather.3.cloned.1.call-update) | async-done | bytes 2097168 | tf_op jit(solution)/shard_map/all_gather | solution.py:55
  59.3 5.6 %multiply_convert_fusion.4 = (bf16[512,768]{1,0:T(8,128)(2,1)S(1)}, bf16[512,768]{1,0:T(8,128)(2,1)S(1)}) fusion(f32[512,768]{1,0:T(8,128)} %fusion.2, f32[512,768]{1,0:T(8,128)} %fusion.6, bf16[1,768,2048]{2,1,0:T(8,128)(2,1)} %param.19, bf16[1,512,2048]{2,1,0:T(8,128)(2,1)} %all-gather.3.cloned.1.call-done), kind=kOutput, calls=%fused_computation.25 | convolution fusion | flops 1615724544 | bytes 9961472 | tf_op jit(solution)/shard_map/dot_general | solution.py:28
  65.0 1.8 fusion
  67.4 3.1 %fusion.15 = bf16[1,512,2048]{2,1,0:T(8,128)(2,1)} fusion(f32[512,2048]{1,0:T(8,128)S(1)} %fusion, bf16[512,768]{1,0:T(8,128)(2,1)S(1)} %get-tuple-element.42, bf16[1,2048,768]{2,1,0:T(8,128)(2,1)S(1)} %copy-done.10), kind=kOutput, calls=%fused_computation.17 | convolution fusion | flops 1612709888 | bytes 10223616 | tf_op jit(solution)/shard_map/dot_general | solution.py:28
  70.8 31.1 %reduce-scatter.2.cloned.1.call-done = bf16[1,512,512]{2,1,0:T(8,128)(2,1)} async-done(((bf16[1,512,2048]{2,1,0:T(8,128)(2,1)}), bf16[1,512,512]{2,1,0:T(8,128)(2,1)}) %reduce-scatter.2.cloned.1.call-update) | async-done | bytes 524304 | tf_op jit(solution)/shard_map/reduce_scatter | solution.py:63
  101.9 1.5 fusion.43
  113.7 5.5 %all-to-all-start.1 = ((bf16[8,1,64,512]{3,2,1,0:T(8,128)(2,1)}), bf16[8,1,64,512]{3,2,1,0:T(8,128)(2,1)}, u32[]{:S(2)}, u32[]{:S(2)}) async-start(bf16[8,1,64,512]{3,2,1,0:T(8,128)(2,1)} %fusion.36), calls=%async_computation.2 | async-start | bytes 1048576 | tf_op jit(solution)/shard_map/all_to_all | solution.py:67
  119.4 5.4 %fusion.10 = bf16[1,2048,768]{1,2,0:T(8,128)(2,1)} fusion(bf16[512,768]{1,0:T(8,128)(2,1)} %copy-done.13, bf16[1,512,2048]{2,1,0:T(8,128)(2,1)} %param.16), kind=kOutput, calls=%fused_computation.14 | convolution fusion | flops 1613758464 | bytes 6029312 | tf_op jit(solution)/shard_map/dot_general | solution.py:22
  124.7 8.9 %all-to-all-done.1 = bf16[8,1,64,512]{3,2,1,0:T(8,128)(2,1)} async-done(((bf16[8,1,64,512]{3,2,1,0:T(8,128)(2,1)}), bf16[8,1,64,512]{3,2,1,0:T(8,128)(2,1)}, u32[]{:S(2)}, u32[]{:S(2)}) %all-to-all-start.1) | async-done | bytes 524320 | tf_op jit(solution)/shard_map/all_to_all | solution.py:67
  134.9 6.7 %all_gather.10 = bf16[128,2048]{1,0:T(8,128)(2,1)S(1)} all-gather(bf16[128,512]{1,0:T(8,128)(2,1)S(1)} %fusion.25), channel_id=1, replica_groups=mesh['sp'=8,'tp'=4] {'tp'}, dimensions={1}, use_global_device_ids=true | all-gather | bytes 655360 | tf_op jit(solution)/shard_map/all_gather | solution.py:122
  142.4 2.8 %fusion.29 = (bf16[128,512]{1,0:T(8,128)(2,1)S(1)}, bf16[128,512]{1,0:T(8,128)(2,1)}, bf16[128,512]{1,0:T(8,128)(2,1)}) fusion(bf16[128,512]{1,0:T(8,128)(2,1)} %param.20, bf16[128,512]{1,0:T(8,128)(2,1)} %param.23, bf16[128,2048]{1,0:T(8,128)(2,1)S(1)} %all_gather.10, bf16[2048,512]{1,0:T(8,128)(2,1)} %param.25), kind=kOutput, calls=%fused_computation.42 | convolution fusion | flops 268959744 | bytes 3276800 | tf_op jit(solution)/shard_map/dot_general | solution.py:123
  145.2 6.1 %fusion.12 = bf16[1,768,2048]{2,1,0:T(8,128)(2,1)} fusion(bf16[1,512,2048]{2,1,0:T(8,128)(2,1)} %all-gather.3.cloned.1.call-done, f32[512,768]{1,0:T(8,128)} %fusion.6, f32[512,768]{1,0:T(8,128)} %fusion.2), kind=kOutput, calls=%fused_computation.16 | convolution fusion | flops 1616117760 | bytes 8388608 | tf_op jit(solution)/shard_map/dot_general | solution.py:22
  152.2 4.2 %all-to-all-start.2 = ((bf16[128,8,256]{2,0,1:T(8,128)(2,1)}), bf16[128,8,256]{2,0,1:T(8,128)(2,1)}, u32[]{:S(2)}, u32[]{:S(2)}) async-start(bf16[128,8,256]{2,0,1:T(8,128)(2,1)} %bitcast.111), calls=%async_computation.3 | async-start | bytes 1048576 | tf_op jit(solution)/shard_map/all_to_all | solution.py:135
  157.0 3.8 %collective-permute-start = (bf16[1,512]{1,0:T(2,128)(2,1)}, bf16[1,512]{1,0:T(2,128)(2,1)S(1)}, u32[]{:S(2)}, u32[]{:S(2)}) collective-permute-start(bf16[1,512]{1,0:T(2,128)(2,1)} %get-tuple-element.47), channel_id=1, source_target_pairs={{0,4},{4,8},{8,12},{12,16},{16,20},{20,24},{24,28},{1,5},{5,9},{9,... | collective-permute-start | bytes 3080 | tf_op jit(solution)/shard_map/ppermute | solution.py:15
  162.0 5.3 %fusion.11 = bf16[1,2048,768]{1,2,0:T(8,128)(2,1)} fusion(bf16[512,768]{1,0:T(8,128)(2,1)} %copy-done.12, bf16[1,512,2048]{2,1,0:T(8,128)(2,1)} %param.16), kind=kOutput, calls=%fused_computation.15 | convolution fusion | flops 1613758464 | bytes 6029312 | tf_op jit(solution)/shard_map/dot_general | solution.py:22
  167.4 4.6 %copy.46 = bf16[1,2048,768]{2,1,0:T(8,128)(2,1)} copy(bf16[1,2048,768]{1,2,0:T(8,128)(2,1)} %fusion.10) | data formatting | bytes 6291456
  172.0 4.8 %copy.47 = bf16[1,2048,768]{2,1,0:T(8,128)(2,1)} copy(bf16[1,2048,768]{1,2,0:T(8,128)(2,1)} %fusion.11) | data formatting | bytes 6291456
  179.0 9.3 %all-gather.5.cloned.1.call-done = bf16[1024,512]{1,0:T(8,128)(2,1)} async-done(((bf16[128,512]{1,0:T(8,128)(2,1)}), bf16[1024,512]{1,0:T(8,128)(2,1)}) %all-gather.5.cloned.1.call-update) | async-done | bytes 1048592 | tf_op jit(solution)/shard_map/all_gather | solution.py:136
  188.3 2.6 %convolution_multiply_fusion = f32[256,512]{1,0:T(8,128)} fusion(bf16[1024,256]{1,0:T(8,128)(2,1)} %bitcast.23, bf16[1024,512]{1,0:T(8,128)(2,1)} %all-gather.5.cloned.1.call-done), kind=kOutput, calls=%fused_computation.30 | convolution fusion | flops 268566528 | bytes 2097152 | tf_op jit(solution)/shard_map/dot_general | solution.py:22
  (69 shorter events, 22.9 us)
Async XLA Ops:
  7.2 30.4 %copy-start = (bf16[1,2048,768]{2,1,0:T(8,128)(2,1)S(1)}, bf16[1,2048,768]{2,1,0:T(8,128)(2,1)}, u32[]{:S(2)}) copy-start(bf16[1,2048,768]{2,1,0:T(8,128)(2,1)} %param.17) | copy-start | bytes 9437188
  7.2 52.1 %all-gather.3.cloned.1.call-start = ((), (), s32[]{:S(2)}) async-start(), calls=%async_computation.4 | async-start | bytes 2621440 | tf_op jit(solution)/shard_map/all_gather | solution.py:55
  37.6 64.3 %reduce-scatter.2.cloned.1.call-start = ((), (), s32[]{:S(2)}) async-start(), calls=%async_computation.5 | async-start | bytes 2621440 | tf_op jit(solution)/shard_map/reduce_scatter | solution.py:63
  37.6 4.7 %copy-start.9 = (bf16[1,2048,768]{2,1,0:T(8,128)(2,1)S(1)}, bf16[1,2048,768]{2,1,0:T(8,128)(2,1)}, u32[]{:S(2)}) copy-start(bf16[1,2048,768]{2,1,0:T(8,128)(2,1)} %param.18) | copy-start | bytes 9437188
  37.6 4.7 %copy-start.11 = (bf16[1,512,2048]{2,1,0:T(8,128)(2,1)S(1)}, bf16[1,512,2048]{2,1,0:T(8,128)(2,1)}, u32[]{:S(2)}) copy-start(bf16[1,512,2048]{2,1,0:T(8,128)(2,1)} %param.16) | copy-start | bytes 6291460
  64.9 1.9 copy-start.13
  64.9 1.9 copy-start.12
  64.9 2.5 %copy-start.10 = (bf16[1,2048,768]{2,1,0:T(8,128)(2,1)S(1)}, bf16[1,2048,768]{2,1,0:T(8,128)(2,1)}, u32[]{:S(2)}) copy-start(bf16[1,2048,768]{2,1,0:T(8,128)(2,1)} %param.18) | copy-start | bytes 9437188
  70.5 48.7 %copy-start.8 = (s32[128,2]{0,1:T(2,128)S(1)}, s32[128,2]{0,1:T(2,128)}, u32[]{:S(2)}) copy-start(s32[128,2]{0,1:T(2,128)} %param.14) | copy-start | bytes 3076
  70.5 48.8 %copy-start.7 = (bf16[3,512]{1,0:T(4,128)(2,1)S(1)}, bf16[3,512]{1,0:T(4,128)(2,1)}, u32[]{:S(2)}) copy-start(bf16[3,512]{1,0:T(4,128)(2,1)} %param.24) | copy-start | bytes 9220
  113.7 19.9 %all-to-all-start.1 = ((bf16[8,1,64,512]{3,2,1,0:T(8,128)(2,1)}), bf16[8,1,64,512]{3,2,1,0:T(8,128)(2,1)}, u32[]{:S(2)}, u32[]{:S(2)}) async-start(bf16[8,1,64,512]{3,2,1,0:T(8,128)(2,1)} %fusion.36), calls=%async_computation.2 | async-start | bytes 1048576 | tf_op jit(solution)/shard_map/all_to_all | solution.py:67
  119.2 69.1 %all-gather.5.cloned.1.call-start = ((), (), s32[]{:S(2)}) async-start(), calls=%async_computation.6 | async-start | bytes 1179648 | tf_op jit(solution)/shard_map/all_gather | solution.py:136
  119.3 14.3 %copy-start.3 = (bf16[128,512]{1,0:T(8,128)(2,1)S(1)}, bf16[128,512]{1,0:T(8,128)(2,1)}, u32[]{:S(2)}) copy-start(bf16[128,512]{1,0:T(8,128)(2,1)} %param.13) | copy-start | bytes 393220
  134.9 16.5 %copy-start.4 = (bf16[128,512]{1,0:T(8,128)(2,1)}, bf16[128,512]{1,0:T(8,128)(2,1)S(1)}, u32[]{:S(2)}) copy-start(bf16[128,512]{1,0:T(8,128)(2,1)S(1)} %fusion.25) | copy-start | bytes 393220
  141.6 0.8 copy-start.1
  145.2 6.2 %copy-start.2 = (bf16[128,2048]{1,0:T(8,128)(2,1)S(1)}, bf16[128,2048]{1,0:T(8,128)(2,1)}, u32[]{:S(2)}) copy-start(bf16[128,2048]{1,0:T(8,128)(2,1)} %copy-done.1) | copy-start | bytes 1572868
  152.2 26.8 %all-to-all-start.2 = ((bf16[128,8,256]{2,0,1:T(8,128)(2,1)}), bf16[128,8,256]{2,0,1:T(8,128)(2,1)}, u32[]{:S(2)}, u32[]{:S(2)}) async-start(bf16[128,8,256]{2,0,1:T(8,128)(2,1)} %bitcast.111), calls=%async_computation.3 | async-start | bytes 1048576 | tf_op jit(solution)/shard_map/all_to_all | solution.py:135
  157.0 19.9 %collective-permute-start = (bf16[1,512]{1,0:T(2,128)(2,1)}, bf16[1,512]{1,0:T(2,128)(2,1)S(1)}, u32[]{:S(2)}, u32[]{:S(2)}) collective-permute-start(bf16[1,512]{1,0:T(2,128)(2,1)} %get-tuple-element.47), channel_id=1, source_target_pairs={{0,4},{4,8},{8,12},{12,16},{16,20},{20,24},{24,28},{1,5},{5,9},{9,... | collective-permute-start | bytes 3080 | tf_op jit(solution)/shard_map/ppermute | solution.py:15
  160.7 16.1 %collective-permute-start.1 = (bf16[1,512]{1,0:T(2,128)(2,1)}, bf16[1,512]{1,0:T(2,128)(2,1)}, u32[]{:S(2)}, u32[]{:S(2)}) collective-permute-start(bf16[1,512]{1,0:T(2,128)(2,1)} %get-tuple-element.48), channel_id=1, source_target_pairs={{4,0},{8,4},{12,8},{16,12},{20,16},{24,20},{28,24},{5,1},{9,5},{13... | collective-permute-start | bytes 3080 | tf_op jit(solution)/shard_map/ppermute | solution.py:16
  172.0 5.5 %copy-start.5 = (bf16[128,512]{1,0:T(8,128)(2,1)S(1)}, bf16[128,512]{1,0:T(8,128)(2,1)}, u32[]{:S(2)}) copy-start(bf16[128,512]{1,0:T(8,128)(2,1)} %param.21) | copy-start | bytes 393220
  172.0 6.3 %copy-start.6 = (bf16[128,512]{1,0:T(8,128)(2,1)S(1)}, bf16[128,512]{1,0:T(8,128)(2,1)}, u32[]{:S(2)}) copy-start(bf16[128,512]{1,0:T(8,128)(2,1)} %param.22) | copy-start | bytes 393220
Sparse Core Ops, SparseCore 0:
  37.7 21.5 all-gather.2
  70.7 31.1 reduce-scatter.1
  145.3 42.8 all-gather.4
